TPU v7x, 32 devices: a whole 2x2x4 slice. The times are simulated.
32 devices in a mesh: fs: 8 (over z, y), tp: 4 (over x, core).
Axes of the slice: x: 2, y: 2, z: 4, core: 2. Of those that a mesh axis runs over, the one named last changes fastest.
Arguments:
- resid: bfloat16 [12288, 2048], P(('fs', 'tp')), may hold values from -6 to 6
- norm1_gain: float32 [2048], replicated, may hold values from 0.1 to 1.9
- w_value: float32 [2048, 2048], P('fs', 'tp'), may hold values from -0.125 to 0.125
- w_gate: float32 [2048, 2048], P('fs', 'tp'), may hold values from -0.125 to 0.125
- value_scale: float32 [2048], replicated, may hold values from 0.3 to 3
- gate_scale: float32 [2048], replicated, may hold values from 0.5 to 3
- conv_taps: float32 [31, 2048], replicated, may hold values from -1 to 1
- conv_gain: float32 [2048], replicated, may hold values from 0.1 to 1.9
- w_point: float32 [2048, 2048], P('tp', 'fs'), may hold values from -0.125 to 0.125
- point_scale: float32 [2048], P('fs'), may hold values from 0.5 to 3
- norm2_gain: float32 [2048], replicated, may hold values from 0.1 to 1.9
- w_up: float32 [2048, 8192], P('fs', 'tp'), may hold values from -0.125 to 0.125
- up_scale: float32 [8192], P('tp'), may hold values from 0.5 to 1.5
- w_down: float32 [8192, 2048], P('tp', 'fs'), may hold values from -0.0625 to 0.0625
- down_scale: float32 [2048], P('fs'), may hold values from 0.3 to 1
Outputs:
- layer_out: bfloat16 [12288, 2048], P(('fs', 'tp'))
All inputs are finite; a program needn't handle non-finite values.
Results may differ from a plain program's by a relative error of at most 0.015.
Values may be sent and summed in bfloat16 or wider, within the bound.
A program may use at most 128 MiB of HBM per device.

v0:
```python
import functools

import jax
import jax.numpy as jnp
from jax import lax
from jax.experimental import pallas as pl
from jax.experimental.pallas import tpu as pltpu
from jax.sharding import PartitionSpec as P

GROUPS = 4
CORES = 2
CHUNKS = 16
PIECES = 4
LANES = 128
PAD = 16
MESH = pl.DeviceIdType.MESH


def ring_at(q, count):
    q = lax.rem(q + 2 * count, count)
    high = q // (count // 2)
    return (1 - high) * 2 * q + high * (2 * (count - 1 - q) + 1)


def layer_kernel(
    n, count, group_width,
    resid_hbm, vg_hbm, pt_hbm, up_hbm, dn_hbm, gain1_ref, vs_ref, gs_ref, taps_ref, cgain_ref, gain2_ref, us_ref,
    out_ref,
    resid, tok1, tok2, vg, pt, up, dn, gl, cv, act, pb, near_in, far_in, theirs, st, st_in,
    load_sem, ring_send, ring_recv,
    g1fs, g1fr, g1ns, g1nr, sss, ssr, scns, scnr, scfs, scfr, g2fs, g2fr, g2ns, g2nr, mns, mnr, mfs, mfr,
):
    me = lax.axis_index("tp")
    core = lax.rem(me, CORES)
    chip = me // CORES
    chips = n // CORES
    other = CORES - 1 - core
    partner = chip * CORES + other
    seat = lax.axis_index("fs")
    odd = lax.rem(seat, 2)
    pos = (1 - odd) * (seat // 2) + odd * (count - 1 - seat // 2)
    right, left = ring_at(pos + 1, count), ring_at(pos - 1, count)
    rows, width = resid.shape
    seq = rows * n
    pieces = CHUNKS // n
    r = rows // pieces
    own_w = pt.shape[1]
    blocks = own_w // LANES
    db = pt.shape[2]
    hid = dn.shape[1]
    far_step = count // 2
    reach = taps_ref.shape[0] // 2
    f32 = jnp.float32

    def chip_core(c, k):
        return lax.rem(c + 2 * chips, chips) * CORES + k

    loads = [
        pltpu.make_async_copy(vg_hbm, vg.at[pl.ds(pl.multiple_of(seat * db, db), db)], load_sem.at[0]),
        pltpu.make_async_copy(resid_hbm, resid, load_sem.at[1]),
        pltpu.make_async_copy(pt_hbm, pt.at[seat], load_sem.at[2]),
        pltpu.make_async_copy(up_hbm, up.at[pl.ds(pl.multiple_of(seat * db, db), db)], load_sem.at[3]),
        pltpu.make_async_copy(dn_hbm, dn.at[0], load_sem.at[4]),
    ]
    for load in loads:
        load.start()
    barrier = pltpu.get_barrier_semaphore()
    for target in (left, right):
        pl.semaphore_signal(barrier, inc=1, device_id={"fs": target}, device_id_type=MESH)
    for d in range(1, n):
        pl.semaphore_signal(barrier, inc=1, device_id={"tp": lax.rem(me + d, n)}, device_id_type=MESH)
    pl.semaphore_wait(barrier, n + 1)

    VG, PT, UP, DN = range(4)

    def spot(a, s, k, clockwise):
        owner = ring_at(pos - s if clockwise else pos + s, count)
        if a in (VG, UP):
            step = db // PIECES
            return (vg if a == VG else up).at[pl.ds(pl.multiple_of(owner * db + k * step, step), step)]
        if a == PT:
            step = own_w // PIECES
            return pt.at[owner, pl.ds(pl.multiple_of(k * step, step), step)]
        step = hid // PIECES
        slot = lax.rem(s if clockwise else count - s, count)
        return dn.at[slot, pl.ds(pl.multiple_of(k * step, step), step)]

    def dn_dst(s, k, clockwise):
        step = hid // PIECES
        return dn.at[s if clockwise else count - s, pl.ds(pl.multiple_of(k * step, step), step)]

    def hop(a, s, k, clockwise):
        way = 0 if clockwise else 1
        src = spot(a, s - 1, k, clockwise)
        dst = dn_dst(s, k, clockwise) if a == DN else src
        return pltpu.make_async_remote_copy(
            src_ref=src, dst_ref=dst, send_sem=ring_send.at[a, way, s - 1, k], recv_sem=ring_recv.at[a, way, s - 1, k],
            device_id={"fs": right if clockwise else left}, device_id_type=MESH)

    def arrived(a, s, k, clockwise):
        way = 0 if clockwise else 1
        here = spot(a, s, k, clockwise)
        pltpu.make_async_remote_copy(
            src_ref=here, dst_ref=here, send_sem=ring_send.at[a, way, s - 1, k], recv_sem=ring_recv.at[a, way, s - 1, k],
            device_id={"fs": right if clockwise else left}, device_id_type=MESH).wait_recv()

    half = PIECES // 2
    full_items = (far_step - 1) * PIECES
    items = full_items + half

    def first_hops(a):
        for k in range(PIECES):
            for clockwise in (True, False):
                hop(a, 1, k, clockwise).start()

    def service(a, i):
        if isinstance(i, int) and i >= full_items:
            k = i - full_items
            arrived(a, far_step, k, True)
            arrived(a, far_step, k + half, False)
            return
        s, k = i // PIECES + 1, i % PIECES
        for clockwise in (True, False):
            arrived(a, s, k, clockwise)
            mine = k < half if clockwise else k >= half
            if isinstance(i, int):
                if s + 1 < far_step or mine:
                    hop(a, s + 1, k, clockwise).start()
            else:
                @pl.when(jnp.logical_or(s + 1 < far_step, mine))
                def _():
                    hop(a, s + 1, k, clockwise).start()

    done = [0, 0, 0, 0]

    def upto(a, q):
        q = q * items // 14
        for i in range(done[a], q):
            service(a, i)
            if i == full_items - 1 and a < DN:
                first_hops(a + 1)
        done[a] = max(done[a], q)

    loads[0].wait()
    first_hops(VG)

    loads[1].wait()

    def t1(owner, k):
        return tok1.at[pl.ds(pl.multiple_of(owner * rows + k * r, r), r)]

    def far1(d, k, owner, target):
        return pltpu.make_async_remote_copy(
            src_ref=t1(owner, k), dst_ref=t1(owner, k), send_sem=g1fs.at[d - 1, k], recv_sem=g1fr.at[d - 1, k],
            device_id={"tp": target}, device_id_type=MESH)

    def near1(d, k, owner):
        return pltpu.make_async_remote_copy(
            src_ref=t1(owner, k), dst_ref=t1(owner, k), send_sem=g1ns.at[d, k], recv_sem=g1nr.at[d, k],
            device_id={"tp": partner}, device_id_type=MESH)

    sub = 16
    for k in range(pieces):
        @pl.loop(0, r // sub)
        def _(t):
            at = k * r + t * sub
            data = resid[pl.ds(pl.multiple_of(at, sub), sub), :].astype(f32)
            scale = lax.rsqrt(jnp.mean(data * data, axis=-1, keepdims=True) + 1e-06)
            tok1[pl.ds(pl.multiple_of(me * rows + at, sub), sub), :] = (data * scale * gain1_ref[...]).astype(tok1.dtype)

        for d in range(1, chips):
            far1(d, k, me, chip_core(chip + d, core)).start()
        near1(0, k, me).start()
    for load in loads[2:]:
        load.wait()
    passed = 0
    for q in range(14):
        upto(VG, q + 1)
        while passed < pieces and (passed + 1) * 13 // pieces <= q + 1:
            for d in range(1, chips):
                owner = chip_core(chip - d, core)
                far1(d, passed, owner, partner).wait_recv()
                near1(d, passed, owner).start()
            passed += 1
    for k in range(pieces):
        for d in range(chips):
            near1(d, k, chip_core(chip - d, other)).wait_recv()

    gl[:, 0:PAD, :] = jnp.zeros((blocks, PAD, LANES), f32)
    gl[:, PAD + seq :, :] = jnp.zeros((blocks, PAD, LANES), f32)
    mine_w = pl.multiple_of(me * own_w, own_w)
    tile = 256
    tiles = seq // tile
    wide = 2 * LANES

    @pl.loop(0, tiles)
    def _(t):
        at = pl.multiple_of(t * tile, tile)
        for c in range(0, own_w, wide):
            lhs = tok1[pl.ds(at, tile), :]
            value = jnp.dot(lhs, vg[:, c : c + wide], preferred_element_type=f32)
            gate = jnp.dot(lhs, vg[:, own_w + c : own_w + c + wide], preferred_element_type=f32)
            value = value * vs_ref[:, pl.ds(mine_w + c, wide)]
            gate = gate * gs_ref[:, pl.ds(mine_w + c, wide)]
            glu = (value * jax.nn.sigmoid(gate)).astype(jnp.bfloat16).astype(f32)
            for b in range(wide // LANES):
                gl[c // LANES + b, pl.ds(PAD + at, tile), :] = glu[:, b * LANES : (b + 1) * LANES]

        @pl.when(jnp.logical_and(t >= 2, t < 2 + PIECES))
        def _():
            service(PT, t - 2)

    done[PT] = PIECES

    span = seq // CHUNKS
    lane = lax.broadcasted_iota(jnp.int32, (span, LANES), 1)
    st[...] = jnp.zeros(st.shape, f32)

    def spread(v, width_from):
        while width_from < LANES:
            v = v + pltpu.roll(v, width_from, 1)
            width_from *= 2
        return v

    @pl.loop(0, CHUNKS)
    def _(i):
        at = pl.multiple_of(i * span, span)
        total = jnp.zeros((span, LANES), f32)
        square = jnp.zeros((span, LANES), f32)
        for b in range(blocks):
            window = gl[b, pl.ds(at, span + 2 * PAD), :]
            lanes = pl.ds(mine_w + b * LANES, LANES)
            conv = None
            for phase in range(8):
                acc = None
                for a in range(4):
                    j = 8 * a + phase + reach - PAD
                    if j < 0 or j > 2 * reach:
                        continue
                    term = taps_ref[j : j + 1, lanes] * window[8 * a : 8 * a + span + 8]
                    acc = term if acc is None else acc + term
                if phase:
                    acc = pltpu.roll(acc, span + 8 - phase, 0)
                acc = acc[:span]
                conv = acc if conv is None else conv + acc
            cv[b, pl.ds(at, span), :] = conv
            total = total + conv
            square = square + conv * conv
        total = spread(total, GROUPS)
        square = spread(square, GROUPS)
        here = lane // (2 * GROUPS) == i
        st[...] = jnp.where(here, jnp.where(lane % (2 * GROUPS) < GROUPS, total, square), st[...])

        @pl.when(jnp.logical_and(i >= 6, i < 6 + 2 * PIECES))
        def _():
            service(PT, PIECES + i - 6)

    done[PT] = 3 * PIECES
    if full_items == 3 * PIECES:
        first_hops(UP)

    def stat(d):
        return pltpu.make_async_remote_copy(
            src_ref=st, dst_ref=st_in.at[d - 1], send_sem=sss.at[d - 1], recv_sem=ssr.at[d - 1],
            device_id={"tp": lax.rem(me + d, n)}, device_id_type=MESH)

    for d in range(1, n):
        stat(d).start()
    upto(PT, 14)
    for d in range(1, n):
        stat(d).wait_recv()
    for d in range(1, n):
        stat(d).wait_send()
    st_sum = st[...]
    for d in range(1, n):
        st_sum = st_sum + st_in[d - 1]
    st[...] = st_sum

    def scn(d, k):
        return pltpu.make_async_remote_copy(
            src_ref=pb.at[:, k, chip_core(chip + d, other)],
            dst_ref=near_in.at[:, k] if d == 0 else theirs.at[d - 1, :, k],
            send_sem=scns.at[d, k], recv_sem=scnr.at[d, k], device_id={"tp": partner}, device_id_type=MESH)

    def scf(d, k):
        return pltpu.make_async_remote_copy(
            src_ref=pb.at[:, k, chip_core(chip + d, core)], dst_ref=far_in.at[d - 1, :, k],
            send_sem=scfs.at[d - 1, k], recv_sem=scfr.at[d - 1, k],
            device_id={"tp": chip_core(chip + d, core)}, device_id_type=MESH)

    def mix(k):
        @pl.loop(0, n)
        def _(o):
            i = o * pieces + k
            here = lane // GROUPS
            stats = st[...]
            gmean = spread(jnp.where(here == 2 * i, stats, 0.0), GROUPS) / group_width
            gsquare = spread(jnp.where(here == 2 * i + 1, stats, 0.0), GROUPS) / group_width
            inv = lax.rsqrt(gsquare - gmean * gmean + 1e-05)
            for b in range(blocks):
                conv = cv[b, pl.ds(pl.multiple_of(i * span, span), span), :]
                scaled = (conv - gmean) * inv * cgain_ref[:, pl.ds(mine_w + b * LANES, LANES)]
                act[pl.ds(pl.multiple_of((k * n + o) * r, r), r), b * LANES : (b + 1) * LANES] = (
                    scaled / (1.0 + jnp.exp(-scaled))
                ).astype(act.dtype)

        @pl.loop(0, count)
        def _(j):
            part = jnp.dot(act[k * n * r : (k + 1) * n * r, :], pt[j], preferred_element_type=f32)
            pb[j, k] = part.astype(pb.dtype).reshape(n, r, db)

        for d in list(range(1, chips)) + [0]:
            scn(d, k).start()

    def mix_far(k):
        for d in range(1, chips):
            scn(d, k).wait_recv()
            owner = chip_core(chip + d, core)

            @pl.loop(0, count)
            def _(j):
                total = pb[j, k, owner].astype(f32) + theirs[d - 1, j, k].astype(f32)
                pb[j, k, owner] = total.astype(pb.dtype)

            scf(d, k).start()

    def t2(owner, k):
        return tok2.at[k, owner]

    def far2(d, k, owner, target):
        return pltpu.make_async_remote_copy(
            src_ref=t2(owner, k), dst_ref=t2(owner, k), send_sem=g2fs.at[d - 1, k], recv_sem=g2fr.at[d - 1, k],
            device_id={"tp": target}, device_id_type=MESH)

    def near2(d, k, owner):
        return pltpu.make_async_remote_copy(
            src_ref=t2(owner, k), dst_ref=t2(owner, k), send_sem=g2ns.at[d, k], recv_sem=g2nr.at[d, k],
            device_id={"tp": partner}, device_id_type=MESH)

    def mix_end(k):
        scn(0, k).wait_recv()
        for d in range(1, chips):
            scf(d, k).wait_recv()

        @pl.loop(0, r // sub)
        def _(t):
            at = pl.multiple_of(t * sub, sub)
            mid_at = pl.ds(pl.multiple_of(k * r + at, sub), sub)
            power = jnp.zeros((sub, 1), f32)
            mids = []
            for j in range(count):
                total = pb[j, k, me, pl.ds(at, sub), :].astype(f32) + near_in[j, k, pl.ds(at, sub), :].astype(f32)
                for d in range(1, chips):
                    total = total + far_in[d - 1, j, k, pl.ds(at, sub), :].astype(f32)
                cols = slice(j * db, (j + 1) * db)
                middle = (resid[mid_at, cols].astype(f32) + total).astype(out_ref.dtype)
                out_ref[mid_at, cols] = middle
                middle = middle.astype(f32)
                power = power + jnp.sum(middle * middle, axis=-1, keepdims=True)
                mids.append(middle)
            scale = lax.rsqrt(power / width + 1e-06)
            for j in range(count):
                cols = slice(j * db, (j + 1) * db)
                tok2[k, me, pl.ds(at, sub), cols] = (mids[j] * scale * gain2_ref[:, cols]).astype(tok2.dtype)

        for d in range(1, chips):
            far2(d, k, me, chip_core(chip + d, core)).start()
        near2(0, k, me).start()

    def gather_pass(k):
        for d in range(1, chips):
            owner = chip_core(chip - d, core)
            far2(d, k, owner, partner).wait_recv()
            near2(d, k, owner).start()

    for k in range(pieces):
        mix(k)
        if k:
            mix_far(k - 1)
    mix_far(pieces - 1)
    plan = [3, 5, 7, 9]
    for k in range(pieces):
        mix_end(k)
        upto(UP, plan[k * 4 // pieces])
    plan = [10, 12, 13, 14]
    for k in range(pieces):
        gather_pass(k)
        upto(UP, plan[(k + 1) * 4 // pieces - 1])

    for k in range(pieces):
        for d in range(1, chips):
            far1(d, k, me, partner).wait_send()
        for d in range(chips):
            near1(d, k, me).wait_send()
    block = min(512, hid)
    group = n * r

    def expand(k):
        for d in range(chips):
            near2(d, k, chip_core(chip - d, other)).wait_recv()

        @pl.loop(0, hid // block)
        def _(c):
            cols = pl.ds(pl.multiple_of(c * block, block), block)
            lhs = tok2[k].reshape(group, width)
            upper = jnp.dot(lhs, up[:, cols], preferred_element_type=f32)
            upper = jnp.maximum(upper * us_ref[:, cols], 0.0)
            tok1[k * group : (k + 1) * group, cols] = (upper * upper).astype(tok1.dtype)

    for k in range(pieces):
        expand(k)
        upto(DN, k * 4 // pieces)

    for k in range(pieces):
        for d in range(chips):
            scn(d, k).wait_send()
        for d in range(1, chips):
            scf(d, k).wait_send()

    def near(j, d):
        return pltpu.make_async_remote_copy(
            src_ref=pb.at[j, :, chip_core(chip + d, other)], dst_ref=near_in.at[j] if d == 0 else theirs.at[d - 1, j],
            send_sem=mns.at[j, d], recv_sem=mnr.at[j, d], device_id={"tp": partner}, device_id_type=MESH)

    def far(j, d):
        return pltpu.make_async_remote_copy(
            src_ref=pb.at[j, :, chip_core(chip + d, core)], dst_ref=far_in.at[d - 1, j],
            send_sem=mfs.at[j, d - 1], recv_sem=mfr.at[j, d - 1],
            device_id={"tp": chip_core(chip + d, core)}, device_id_type=MESH)

    def contract(j):
        @pl.loop(0, pieces)
        def _(k):
            lhs = tok1[pl.ds(pl.multiple_of(k * group, group), group), 0:hid]
            part = jnp.dot(lhs, dn[j], preferred_element_type=f32)
            pb[j, k] = part.astype(pb.dtype).reshape(n, r, db)

        for d in list(range(1, chips)) + [0]:
            near(j, d).start()

    def combine(j):
        for d in range(1, chips):
            near(j, d).wait_recv()
            owner = chip_core(chip + d, core)

            @pl.loop(0, pieces)
            def _(k):
                total = pb[j, k, owner].astype(f32) + theirs[d - 1, j, k].astype(f32)
                pb[j, k, owner] = total.astype(pb.dtype)

            far(j, d).start()

    def finish(j):
        near(j, 0).wait_recv()
        for d in range(1, chips):
            far(j, d).wait_recv()
        cols = pl.ds(pl.multiple_of(ring_at(pos - j, count) * db, db), db)

        @pl.loop(0, pieces)
        def _(k):
            total = pb[j, k, me].astype(f32) + near_in[j, k].astype(f32)
            for d in range(1, chips):
                total = total + far_in[d - 1, j, k].astype(f32)
            at = pl.ds(pl.multiple_of(k * r, r), r)
            out_ref[at, cols] = (out_ref[at, cols].astype(f32) + total).astype(out_ref.dtype)

    groups = [[0]] + [[s, count - s] if s < far_step else [s] for s in range(1, far_step + 1)]
    for s, slots in enumerate(groups):
        if s:
            for i in range(done[DN], min(s * PIECES, items)):
                service(DN, i)
            done[DN] = max(done[DN], min(s * PIECES, items))
        for j in slots:
            contract(j)
        for j in slots:
            combine(j)
        if s > 1:
            for j in groups[s - 2]:
                finish(j)
    for slots in groups[-2:]:
        for j in slots:
            finish(j)

    for a in range(4):
        for s in range(1, far_step + 1):
            for k in range(PIECES):
                for clockwise in (True, False):
                    if s < far_step or (k < half) == clockwise:
                        hop(a, s, k, clockwise).wait_send()
    for k in range(pieces):
        for d in range(1, chips):
            far2(d, k, me, partner).wait_send()
        for d in range(chips):
            near2(d, k, me).wait_send()
    for j in range(count):
        for d in range(chips):
            near(j, d).wait_send()
        for d in range(1, chips):
            far(j, d).wait_send()


def layer(resid, vg, pt, up, dn, gain1, vs, gs, taps, cgain, gain2, us, n, count, group_width):
    rows, width = resid.shape
    seq = rows * n
    chips = n // CORES
    pieces = CHUNKS // n
    r = rows // pieces
    own_w, db = pt.shape
    hid = dn.shape[0]
    blocks = own_w // LANES
    steps = count // 2
    kind = resid.dtype
    f32 = jnp.float32
    dma = pltpu.SemaphoreType.DMA
    hbm = pl.BlockSpec(memory_space=pl.ANY)
    vmem = pl.BlockSpec(memory_space=pltpu.VMEM)
    return pl.pallas_call(
        functools.partial(layer_kernel, n, count, group_width),
        out_shape=jax.ShapeDtypeStruct(resid.shape, kind),
        in_specs=[hbm] * 5 + [vmem] * 7,
        out_specs=vmem,
        scratch_shapes=[
            pltpu.VMEM((rows, width), kind),
            pltpu.VMEM((seq, max(width, hid)), kind),
            pltpu.VMEM((pieces, n, r, width), kind),
            pltpu.VMEM((width, 2 * own_w), kind),
            pltpu.VMEM((count, own_w, db), kind),
            pltpu.VMEM((width, hid), kind),
            pltpu.VMEM((count, hid, db), kind),
            pltpu.VMEM((blocks, seq + 2 * PAD, LANES), f32),
            pltpu.VMEM((blocks, seq, LANES), f32),
            pltpu.VMEM((seq, own_w), kind),
            pltpu.VMEM((count, pieces, n, r, db), kind),
            pltpu.VMEM((count, pieces, r, db), kind),
            pltpu.VMEM((chips - 1, count, pieces, r, db), kind),
            pltpu.VMEM((chips - 1, count, pieces, r, db), kind),
            pltpu.VMEM((seq // CHUNKS, LANES), f32),
            pltpu.VMEM((n - 1, seq // CHUNKS, LANES), f32),
            dma((5,)),
            dma((4, 2, steps, PIECES)), dma((4, 2, steps, PIECES)),
            dma((chips - 1, pieces)), dma((chips - 1, pieces)), dma((chips, pieces)), dma((chips, pieces)),
            dma((n - 1,)), dma((n - 1,)),
            dma((chips, pieces)), dma((chips, pieces)), dma((chips - 1, pieces)), dma((chips - 1, pieces)),
            dma((chips - 1, pieces)), dma((chips - 1, pieces)), dma((chips, pieces)), dma((chips, pieces)),
            dma((count, chips)), dma((count, chips)), dma((count, chips - 1)), dma((count, chips - 1)),
        ],
        compiler_params=pltpu.CompilerParams(
            collective_id=1, has_side_effects=True, vmem_limit_bytes=67043328
        ),
        cost_estimate=pl.CostEstimate(flops=8 * seq * hid * width, bytes_accessed=8 * seq * width, transcendentals=0),
        name="layer",
    )(resid, vg, pt, up, dn, gain1.reshape(1, -1), vs.reshape(1, -1), gs.reshape(1, -1), taps,
      cgain.reshape(1, -1), gain2.reshape(1, -1), us.reshape(1, -1))


def shards(
    resid,
    norm1_gain,
    w_value,
    w_gate,
    value_scale,
    gate_scale,
    conv_taps,
    conv_gain,
    w_point,
    point_scale,
    norm2_gain,
    w_up,
    up_scale,
    w_down,
    down_scale,
):
    bf = jnp.bfloat16
    vg = jnp.concatenate([w_value.astype(bf), w_gate.astype(bf)], axis=1)
    pt = (w_point * point_scale).astype(bf)
    up = w_up.astype(bf)
    dn = (w_down * down_scale).astype(bf)
    return layer(
        resid, vg, pt, up, dn, norm1_gain, value_scale, gate_scale, conv_taps, conv_gain, norm2_gain, up_scale,
        lax.axis_size("tp"), lax.axis_size("fs"), value_scale.shape[0] // GROUPS,
    )


def solution(mesh):
    in_specs = (
        P(("fs", "tp"), None),
        P(),
        P("fs", "tp"),
        P("fs", "tp"),
        P(),
        P(),
        P(),
        P(),
        P("tp", "fs"),
        P("fs"),
        P(),
        P("fs", "tp"),
        P("tp"),
        P("tp", "fs"),
        P("fs"),
    )
    out_specs = P(("fs", "tp"), None)
    return jax.shard_map(shards, mesh=mesh, in_specs=in_specs, out_specs=out_specs, check_vma=False)
```

profile of v0, /device:TPU:0, one launch (start us, length us, event | category | flops | bytes accessed | tf_op | source)
XLA Modules:
  0.0 255.0 jit_solution(9855518896711858452)
XLA Ops:
  0.0 0.0 copy-start
  0.0 0.0 copy-start.3
  0.0 0.0 copy-start.2
  0.0 1.2 convert_element_type.15
  1.2 1.1 convert_element_type.16
  2.3 0.9 pad_maximum_fusion.vg_hbm
  3.2 0.0 copy-done.3
  3.2 0.0 copy-done.2
  3.2 0.0 copy-start.1
  3.2 0.0 copy-start.4
  3.2 0.7 multiply_convert_fusion.1.pt_hbm
  4.0 0.0 copy-done
  4.0 1.1 convert_element_type.18.up_hbm
  5.1 0.0 copy-done.1
  5.1 0.0 copy-done.4
  5.1 1.2 multiply_convert_fusion.dn_hbm
  6.2 246.0 %layer.1 = bf16[384,2048]{1,0:T(8,128)(2,1)} custom-call(bf16[384,2048]{1,0:T(8,128)(2,1)} %resid_hbm.1, bf16[256,1024]{1,0:T(8,128)(2,1)} %pad_maximum_fusion.vg_hbm, bf16[512,256]{1,0:T(8,128)(2,1)} %multiply_convert_fusion.1.pt_hbm, bf16[256,2048]{1,0:T(8,128)(2,1)} %convert_element_type.18.up_hbm, bf16[2048,256]{1,0:T(8,128)(2,1)} %multiply_convert_fusion.dn_hbm, ...), custom_call_target="tpu_custom_call" | custom-call | flops 51539607552 | bytes 25165824 | tf_op jit(solution)/shard_map/layer/pallas_call | solution.py:517
  252.2 2.7 %copy.17 = bf16[384,2048]{1,0:T(8,128)(2,1)} copy(bf16[384,2048]{1,0:T(8,128)(2,1)} %layer.1) | data formatting | bytes 3145728
Async XLA Ops:
  0.0 4.0 %copy-start = (f32[256,2048]{1,0:T(8,128)S(1)}, f32[256,2048]{1,0:T(8,128)}, u32[]{:S(2)}) copy-start(f32[256,2048]{1,0:T(8,128)} %param.26) | copy-start | bytes 6291460
  0.0 3.2 %copy-start.3 = (f32[256]{0:T(256)S(1)}, f32[256]{0:T(256)}, u32[]{:S(2)}) copy-start(f32[256]{0:T(256)} %param.24) | copy-start | bytes 3076
  0.0 3.2 %copy-start.2 = (f32[512,256]{1,0:T(8,128)S(1)}, f32[512,256]{1,0:T(8,128)}, u32[]{:S(2)}) copy-start(f32[512,256]{1,0:T(8,128)} %param.23) | copy-start | bytes 1572868
  3.2 1.9 copy-start.1
  3.2 1.9 copy-start.4
where the time goes:
time: 255 us
  Pallas kernels  246 us (96%)
  other arithmetic  6.2 us (2%)
  local copies, waits for them, and re-layouts  2.75 us (1%)
    pallas_call x1, Pallas kernels, layer(): pl.pallas_call(functools.partial(layer_kernel, n, count, group_width), ou...  246 us

commit v1 on v0

--- a/solution.py
+++ b/solution.py
@@ -24,11 +24,14 @@
 
 def layer_kernel(
     n, count, group_width,
-    resid_hbm, vg_hbm, pt_hbm, up_hbm, dn_hbm, gain1_ref, vs_ref, gs_ref, taps_ref, cgain_ref, gain2_ref, us_ref,
-    out_ref,
-    resid, tok1, tok2, vg, pt, up, dn, gl, cv, act, pb, near_in, far_in, theirs, st, st_in,
+    resid_hbm, wv_hbm, wg_hbm, wp_hbm, wu_hbm, wd_hbm,
+    gain1_hbm, vs_hbm, gs_hbm, taps_hbm, cgain_hbm, ps_hbm, gain2_hbm, us_hbm, ds_hbm,
+    out_hbm,
+    gain1_ref, vs_ref, gs_ref, taps_ref, cgain_ref, ps_ref, gain2_ref, us_ref, ds_ref,
+    mid, store_sem,
+    raw_v, raw_g, raw_p, raw_u, raw_d, resid, tok1, tok2, vg, pt, up, dn, gl, cv, act, pb, near_in, far_in, theirs, st, st_in,
     load_sem, ring_send, ring_recv,
-    g1fs, g1fr, g1ns, g1nr, sss, ssr, scns, scnr, scfs, scfr, g2fs, g2fr, g2ns, g2nr, mns, mnr, mfs, mfr,
+    sss, ssr, scns, scnr, scfs, scfr, gfs, gfr, gns, gnr, mns, mnr, mfs, mfr,
 ):
     me = lax.axis_index("tp")
     core = lax.rem(me, CORES)
@@ -55,20 +58,33 @@
     def chip_core(c, k):
         return lax.rem(c + 2 * chips, chips) * CORES + k
 
-    loads = [
-        pltpu.make_async_copy(vg_hbm, vg.at[pl.ds(pl.multiple_of(seat * db, db), db)], load_sem.at[0]),
-        pltpu.make_async_copy(resid_hbm, resid, load_sem.at[1]),
-        pltpu.make_async_copy(pt_hbm, pt.at[seat], load_sem.at[2]),
-        pltpu.make_async_copy(up_hbm, up.at[pl.ds(pl.multiple_of(seat * db, db), db)], load_sem.at[3]),
-        pltpu.make_async_copy(dn_hbm, dn.at[0], load_sem.at[4]),
-    ]
-    for load in loads:
+    places = ((wv_hbm, raw_v), (wg_hbm, raw_g), (resid_hbm, resid), (gain1_hbm, gain1_ref),
+              (wp_hbm, raw_p), (wu_hbm, raw_u), (wd_hbm, raw_d), (vs_hbm, vs_ref), (gs_hbm, gs_ref),
+              (taps_hbm, taps_ref), (cgain_hbm, cgain_ref), (ps_hbm, ps_ref), (gain2_hbm, gain2_ref),
+              (us_hbm, us_ref), (ds_hbm, ds_ref))
+    loads = [pltpu.make_async_copy(src, dst, load_sem.at[i]) for i, (src, dst) in enumerate(places)]
+    for load in loads[:4]:
         load.start()
     barrier = pltpu.get_barrier_semaphore()
     for target in (left, right):
         pl.semaphore_signal(barrier, inc=1, device_id={"fs": target}, device_id_type=MESH)
     for d in range(1, n):
         pl.semaphore_signal(barrier, inc=1, device_id={"tp": lax.rem(me + d, n)}, device_id_type=MESH)
+
+    sub = 16
+    own_rows = pl.multiple_of(seat * db, db)
+    loads[0].wait()
+    loads[1].wait()
+
+    @pl.loop(0, db // sub)
+    def _(t):
+        src = pl.ds(pl.multiple_of(t * sub, sub), sub)
+        dst = pl.ds(pl.multiple_of(own_rows + t * sub, sub), sub)
+        vg[dst, 0:own_w] = raw_v[src, :].astype(vg.dtype)
+        vg[dst, own_w : 2 * own_w] = raw_g[src, :].astype(vg.dtype)
+
+    for load in loads[4:]:
+        load.start()
     pl.semaphore_wait(barrier, n + 1)
 
     VG, PT, UP, DN = range(4)
@@ -91,27 +107,40 @@
 
     def hop(a, s, k, clockwise):
         way = 0 if clockwise else 1
+        turn = (s - 1) % 2
         src = spot(a, s - 1, k, clockwise)
         dst = dn_dst(s, k, clockwise) if a == DN else src
         return pltpu.make_async_remote_copy(
-            src_ref=src, dst_ref=dst, send_sem=ring_send.at[a, way, s - 1, k], recv_sem=ring_recv.at[a, way, s - 1, k],
+            src_ref=src, dst_ref=dst, send_sem=ring_send.at[a % 2, way, turn, k], recv_sem=ring_recv.at[a % 2, way, turn, k],
             device_id={"fs": right if clockwise else left}, device_id_type=MESH)
 
     def arrived(a, s, k, clockwise):
         way = 0 if clockwise else 1
+        turn = (s - 1) % 2
         here = spot(a, s, k, clockwise)
         pltpu.make_async_remote_copy(
-            src_ref=here, dst_ref=here, send_sem=ring_send.at[a, way, s - 1, k], recv_sem=ring_recv.at[a, way, s - 1, k],
+            src_ref=here, dst_ref=here, send_sem=ring_send.at[a % 2, way, turn, k], recv_sem=ring_recv.at[a % 2, way, turn, k],
             device_id={"fs": right if clockwise else left}, device_id_type=MESH).wait_recv()
 
     half = PIECES // 2
     full_items = (far_step - 1) * PIECES
     items = full_items + half
 
+    def first_hop(a, k):
+        if a >= 2:
+            drain(a - 2, k)
+        for clockwise in (True, False):
+            hop(a, 1, k, clockwise).start()
+
     def first_hops(a):
         for k in range(PIECES):
-            for clockwise in (True, False):
-                hop(a, 1, k, clockwise).start()
+            first_hop(a, k)
+
+    def drain(a, k):
+        for clockwise in (True, False):
+            last_step = far_step if (k < half) == clockwise else far_step - 1
+            for s in range(max(1, last_step - 1), last_step + 1):
+                hop(a, s, k, clockwise).wait_send()
 
     def service(a, i):
         if isinstance(i, int) and i >= full_items:
@@ -122,11 +151,18 @@
         s, k = i // PIECES + 1, i % PIECES
         for clockwise in (True, False):
             arrived(a, s, k, clockwise)
+        for clockwise in (True, False):
             mine = k < half if clockwise else k >= half
             if isinstance(i, int):
                 if s + 1 < far_step or mine:
+                    if s > 1:
+                        hop(a, s - 1, k, clockwise).wait_send()
                     hop(a, s + 1, k, clockwise).start()
             else:
+                @pl.when(jnp.logical_and(s > 1, jnp.logical_or(s + 1 < far_step, mine)))
+                def _():
+                    hop(a, s - 1, k, clockwise).wait_send()
+
                 @pl.when(jnp.logical_or(s + 1 < far_step, mine))
                 def _():
                     hop(a, s + 1, k, clockwise).start()
@@ -141,25 +177,24 @@
                 first_hops(a + 1)
         done[a] = max(done[a], q)
 
-    loads[0].wait()
     first_hops(VG)
 
-    loads[1].wait()
+    loads[2].wait()
+    loads[3].wait()
 
     def t1(owner, k):
         return tok1.at[pl.ds(pl.multiple_of(owner * rows + k * r, r), r)]
 
     def far1(d, k, owner, target):
         return pltpu.make_async_remote_copy(
-            src_ref=t1(owner, k), dst_ref=t1(owner, k), send_sem=g1fs.at[d - 1, k], recv_sem=g1fr.at[d - 1, k],
+            src_ref=t1(owner, k), dst_ref=t1(owner, k), send_sem=gfs.at[d - 1, k], recv_sem=gfr.at[d - 1, k],
             device_id={"tp": target}, device_id_type=MESH)
 
     def near1(d, k, owner):
         return pltpu.make_async_remote_copy(
-            src_ref=t1(owner, k), dst_ref=t1(owner, k), send_sem=g1ns.at[d, k], recv_sem=g1nr.at[d, k],
+            src_ref=t1(owner, k), dst_ref=t1(owner, k), send_sem=gns.at[d, k], recv_sem=gnr.at[d, k],
             device_id={"tp": partner}, device_id_type=MESH)
 
-    sub = 16
     for k in range(pieces):
         @pl.loop(0, r // sub)
         def _(t):
@@ -171,8 +206,24 @@
         for d in range(1, chips):
             far1(d, k, me, chip_core(chip + d, core)).start()
         near1(0, k, me).start()
-    for load in loads[2:]:
+    for load in loads[4:]:
         load.wait()
+
+    @pl.loop(0, own_w // sub)
+    def _(t):
+        at = pl.ds(pl.multiple_of(t * sub, sub), sub)
+        pt[seat, at, :] = (raw_p[at, :] * ps_ref[...]).astype(pt.dtype)
+
+    @pl.loop(0, db // sub)
+    def _(t):
+        up[pl.ds(pl.multiple_of(own_rows + t * sub, sub), sub), :] = raw_u[
+            pl.ds(pl.multiple_of(t * sub, sub), sub), :].astype(up.dtype)
+
+    @pl.loop(0, hid // sub)
+    def _(t):
+        at = pl.ds(pl.multiple_of(t * sub, sub), sub)
+        dn[0, at, :] = (raw_d[at, :] * ds_ref[...]).astype(dn.dtype)
+
     passed = 0
     for q in range(14):
         upto(VG, q + 1)
@@ -206,11 +257,11 @@
             for b in range(wide // LANES):
                 gl[c // LANES + b, pl.ds(PAD + at, tile), :] = glu[:, b * LANES : (b + 1) * LANES]
 
-        @pl.when(jnp.logical_and(t >= 2, t < 2 + PIECES))
+        @pl.when(jnp.logical_and(t >= 1, t < 2 + PIECES))
         def _():
-            service(PT, t - 2)
-
-    done[PT] = PIECES
+            service(PT, t - 1)
+
+    done[PT] = PIECES + 1
 
     span = seq // CHUNKS
     lane = lax.broadcasted_iota(jnp.int32, (span, LANES), 1)
@@ -251,13 +302,16 @@
         here = lane // (2 * GROUPS) == i
         st[...] = jnp.where(here, jnp.where(lane % (2 * GROUPS) < GROUPS, total, square), st[...])
 
-        @pl.when(jnp.logical_and(i >= 6, i < 6 + 2 * PIECES))
+        @pl.when(jnp.logical_and(i < 11, i % 3 > 0))
         def _():
-            service(PT, PIECES + i - 6)
+            service(PT, PIECES + i // 3 * 2 + i % 3)
+
+        if full_items == 3 * PIECES:
+            @pl.when(i == 10)
+            def _():
+                first_hops(UP)
 
     done[PT] = 3 * PIECES
-    if full_items == 3 * PIECES:
-        first_hops(UP)
 
     def stat(d):
         return pltpu.make_async_remote_copy(
@@ -267,6 +321,11 @@
     for d in range(1, n):
         stat(d).start()
     upto(PT, 14)
+    for k in range(pieces):
+        for d in range(1, chips):
+            far1(d, k, me, partner).wait_send()
+        for d in range(chips):
+            near1(d, k, me).wait_send()
     for d in range(1, n):
         stat(d).wait_recv()
     for d in range(1, n):
@@ -329,12 +388,12 @@
 
     def far2(d, k, owner, target):
         return pltpu.make_async_remote_copy(
-            src_ref=t2(owner, k), dst_ref=t2(owner, k), send_sem=g2fs.at[d - 1, k], recv_sem=g2fr.at[d - 1, k],
+            src_ref=t2(owner, k), dst_ref=t2(owner, k), send_sem=gfs.at[d - 1, k], recv_sem=gfr.at[d - 1, k],
             device_id={"tp": target}, device_id_type=MESH)
 
     def near2(d, k, owner):
         return pltpu.make_async_remote_copy(
-            src_ref=t2(owner, k), dst_ref=t2(owner, k), send_sem=g2ns.at[d, k], recv_sem=g2nr.at[d, k],
+            src_ref=t2(owner, k), dst_ref=t2(owner, k), send_sem=gns.at[d, k], recv_sem=gnr.at[d, k],
             device_id={"tp": partner}, device_id_type=MESH)
 
     def mix_end(k):
@@ -353,8 +412,8 @@
                 for d in range(1, chips):
                     total = total + far_in[d - 1, j, k, pl.ds(at, sub), :].astype(f32)
                 cols = slice(j * db, (j + 1) * db)
-                middle = (resid[mid_at, cols].astype(f32) + total).astype(out_ref.dtype)
-                out_ref[mid_at, cols] = middle
+                middle = (resid[mid_at, cols].astype(f32) + total).astype(mid.dtype)
+                mid[mid_at, cols] = middle
                 middle = middle.astype(f32)
                 power = power + jnp.sum(middle * middle, axis=-1, keepdims=True)
                 mids.append(middle)
@@ -377,21 +436,12 @@
         mix(k)
         if k:
             mix_far(k - 1)
+        upto(UP, min(k * 4 // pieces + 1, 3))
     mix_far(pieces - 1)
-    plan = [3, 5, 7, 9]
+    plan = [4, 6, 7, 9]
     for k in range(pieces):
         mix_end(k)
         upto(UP, plan[k * 4 // pieces])
-    plan = [10, 12, 13, 14]
-    for k in range(pieces):
-        gather_pass(k)
-        upto(UP, plan[(k + 1) * 4 // pieces - 1])
-
-    for k in range(pieces):
-        for d in range(1, chips):
-            far1(d, k, me, partner).wait_send()
-        for d in range(chips):
-            near1(d, k, me).wait_send()
     block = min(512, hid)
     group = n * r
 
@@ -407,7 +457,13 @@
             upper = jnp.maximum(upper * us_ref[:, cols], 0.0)
             tok1[k * group : (k + 1) * group, cols] = (upper * upper).astype(tok1.dtype)
 
-    for k in range(pieces):
+    plan = [10, 12, 14, 14]
+    for k in range(pieces):
+        gather_pass(k)
+        upto(UP, plan[(k + 1) * 4 // pieces - 1])
+        if k == pieces - 2:
+            expand(0)
+    for k in range(1 if pieces > 1 else 0, pieces):
         expand(k)
         upto(DN, k * 4 // pieces)
 
@@ -462,9 +518,60 @@
             for d in range(1, chips):
                 total = total + far_in[d - 1, j, k].astype(f32)
             at = pl.ds(pl.multiple_of(k * r, r), r)
-            out_ref[at, cols] = (out_ref[at, cols].astype(f32) + total).astype(out_ref.dtype)
-
-    groups = [[0]] + [[s, count - s] if s < far_step else [s] for s in range(1, far_step + 1)]
+            mid[at, cols] = (mid[at, cols].astype(f32) + total).astype(mid.dtype)
+
+    last = far_step
+
+    def near_last(k, d):
+        return pltpu.make_async_remote_copy(
+            src_ref=pb.at[last, k, chip_core(chip + d, other)],
+            dst_ref=near_in.at[last, k] if d == 0 else theirs.at[d - 1, last, k],
+            send_sem=scns.at[d, k], recv_sem=scnr.at[d, k], device_id={"tp": partner}, device_id_type=MESH)
+
+    def far_last(k, d):
+        return pltpu.make_async_remote_copy(
+            src_ref=pb.at[last, k, chip_core(chip + d, core)], dst_ref=far_in.at[d - 1, last, k],
+            send_sem=scfs.at[d - 1, k], recv_sem=scfr.at[d - 1, k],
+            device_id={"tp": chip_core(chip + d, core)}, device_id_type=MESH)
+
+    def contract_last(k):
+        lhs = tok1[k * group : (k + 1) * group, 0:hid]
+        part = jnp.dot(lhs, dn[last], preferred_element_type=f32)
+        pb[last, k] = part.astype(pb.dtype).reshape(n, r, db)
+        for d in list(range(1, chips)) + [0]:
+            near_last(k, d).start()
+
+    def combine_last(k):
+        for d in range(1, chips):
+            near_last(k, d).wait_recv()
+            owner = chip_core(chip + d, core)
+            total = pb[last, k, owner].astype(f32) + theirs[d - 1, last, k].astype(f32)
+            pb[last, k, owner] = total.astype(pb.dtype)
+            far_last(k, d).start()
+
+    def finish_last(k):
+        near_last(k, 0).wait_recv()
+        for d in range(1, chips):
+            far_last(k, d).wait_recv()
+        cols = pl.ds(pl.multiple_of(ring_at(pos - last, count) * db, db), db)
+        total = pb[last, k, me].astype(f32) + near_in[last, k].astype(f32)
+        for d in range(1, chips):
+            total = total + far_in[d - 1, last, k].astype(f32)
+        at = slice(k * r, (k + 1) * r)
+        mid[at, cols] = (mid[at, cols].astype(f32) + total).astype(mid.dtype)
+
+    def slots_sent(slots):
+        for j in slots:
+            for d in range(chips):
+                near(j, d).wait_send()
+            for d in range(1, chips):
+                far(j, d).wait_send()
+
+    def store(j):
+        cols = pl.ds(pl.multiple_of(ring_at(pos - j, count) * db, db), db)
+        return pltpu.make_async_copy(mid.at[:, cols], out_hbm.at[:, cols], store_sem.at[j])
+
+    groups = [[0]] + [[s, count - s] for s in range(1, far_step)]
     for s, slots in enumerate(groups):
         if s:
             for i in range(done[DN], min(s * PIECES, items)):
@@ -477,49 +584,77 @@
         if s > 1:
             for j in groups[s - 2]:
                 finish(j)
-    for slots in groups[-2:]:
-        for j in slots:
-            finish(j)
-
-    for a in range(4):
-        for s in range(1, far_step + 1):
+                store(j).start()
+        if s == 1:
             for k in range(PIECES):
-                for clockwise in (True, False):
-                    if s < far_step or (k < half) == clockwise:
-                        hop(a, s, k, clockwise).wait_send()
-    for k in range(pieces):
-        for d in range(1, chips):
-            far2(d, k, me, partner).wait_send()
+                drain(UP, k)
+            for k in range(pieces):
+                for d in range(1, chips):
+                    far2(d, k, me, partner).wait_send()
+                for d in range(chips):
+                    near2(d, k, me).wait_send()
+    for j in groups[-2]:
+        finish(j)
+        store(j).start()
+    upto(DN, 13)
+    for slots in groups[:-1]:
+        slots_sent(slots)
+    upto(DN, 14)
+    for k in range(pieces):
+        contract_last(k)
+        if k:
+            combine_last(k - 1)
+    combine_last(pieces - 1)
+    for j in groups[-1]:
+        finish(j)
+        store(j).start()
+    for k in range(pieces):
+        finish_last(k)
+    store(last).start()
+
+    for k in range(PIECES):
+        drain(DN, k)
+    slots_sent(groups[-1])
+    for k in range(pieces):
         for d in range(chips):
-            near2(d, k, me).wait_send()
+            near_last(k, d).wait_send()
+        for d in range(1, chips):
+            far_last(k, d).wait_send()
     for j in range(count):
-        for d in range(chips):
-            near(j, d).wait_send()
-        for d in range(1, chips):
-            far(j, d).wait_send()
-
-
-def layer(resid, vg, pt, up, dn, gain1, vs, gs, taps, cgain, gain2, us, n, count, group_width):
+        store(j).wait()
+
+
+def layer(resid, wv, wg, wp, wu, wd, gain1, vs, gs, taps, cgain, ps, gain2, us, ds, n, count, group_width):
     rows, width = resid.shape
     seq = rows * n
     chips = n // CORES
     pieces = CHUNKS // n
     r = rows // pieces
-    own_w, db = pt.shape
-    hid = dn.shape[0]
+    own_w, db = wp.shape
+    hid = wd.shape[0]
     blocks = own_w // LANES
-    steps = count // 2
     kind = resid.dtype
     f32 = jnp.float32
     dma = pltpu.SemaphoreType.DMA
     hbm = pl.BlockSpec(memory_space=pl.ANY)
-    vmem = pl.BlockSpec(memory_space=pltpu.VMEM)
+    small = (
+        gain1.reshape(1, -1), vs.reshape(1, -1), gs.reshape(1, -1), taps, cgain.reshape(1, -1), ps.reshape(1, -1),
+        gain2.reshape(1, -1), us.reshape(1, -1), ds.reshape(1, -1),
+    )
     return pl.pallas_call(
         functools.partial(layer_kernel, n, count, group_width),
         out_shape=jax.ShapeDtypeStruct(resid.shape, kind),
-        in_specs=[hbm] * 5 + [vmem] * 7,
-        out_specs=vmem,
+        in_specs=[hbm] * 15,
+        out_specs=hbm,
         scratch_shapes=[
+            *(pltpu.VMEM(x.shape, x.dtype) for x in small),
+            pltpu.VMEM((rows, width), kind),
+            dma((count,)),
+            pltpu.VMEM((db, own_w), f32),
+            pltpu.VMEM((db, own_w), f32),
+            pltpu.VMEM((own_w, db), f32),
+            pltpu.VMEM((db, hid), f32),
+            pltpu.VMEM((hid, db), f32),
             pltpu.VMEM((rows, width), kind),
             pltpu.VMEM((seq, max(width, hid)), kind),
             pltpu.VMEM((pieces, n, r, width), kind),
@@ -536,9 +671,8 @@
             pltpu.VMEM((chips - 1, count, pieces, r, db), kind),
             pltpu.VMEM((seq // CHUNKS, LANES), f32),
             pltpu.VMEM((n - 1, seq // CHUNKS, LANES), f32),
-            dma((5,)),
-            dma((4, 2, steps, PIECES)), dma((4, 2, steps, PIECES)),
-            dma((chips - 1, pieces)), dma((chips - 1, pieces)), dma((chips, pieces)), dma((chips, pieces)),
+            dma((15,)),
+            dma((2, 2, 2, PIECES)), dma((2, 2, 2, PIECES)),
             dma((n - 1,)), dma((n - 1,)),
             dma((chips, pieces)), dma((chips, pieces)), dma((chips - 1, pieces)), dma((chips - 1, pieces)),
             dma((chips - 1, pieces)), dma((chips - 1, pieces)), dma((chips, pieces)), dma((chips, pieces)),
@@ -549,8 +683,7 @@
         ),
         cost_estimate=pl.CostEstimate(flops=8 * seq * hid * width, bytes_accessed=8 * seq * width, transcendentals=0),
         name="layer",
-    )(resid, vg, pt, up, dn, gain1.reshape(1, -1), vs.reshape(1, -1), gs.reshape(1, -1), taps,
-      cgain.reshape(1, -1), gain2.reshape(1, -1), us.reshape(1, -1))
+    )(resid, wv, wg, wp, wu, wd, *small)
 
 
 def shards(
@@ -570,13 +703,9 @@
     w_down,
     down_scale,
 ):
-    bf = jnp.bfloat16
-    vg = jnp.concatenate([w_value.astype(bf), w_gate.astype(bf)], axis=1)
-    pt = (w_point * point_scale).astype(bf)
-    up = w_up.astype(bf)
-    dn = (w_down * down_scale).astype(bf)
     return layer(
-        resid, vg, pt, up, dn, norm1_gain, value_scale, gate_scale, conv_taps, conv_gain, norm2_gain, up_scale,
+        resid, w_value, w_gate, w_point, w_up, w_down,
+        norm1_gain, value_scale, gate_scale, conv_taps, conv_gain, point_scale, norm2_gain, up_scale, down_scale,
         lax.axis_size("tp"), lax.axis_size("fs"), value_scale.shape[0] // GROUPS,
     )
 

time: 255 us -> 240 us (0.941)
  Pallas kernels: 246 us -> 237 us
  other arithmetic: 6.2 us -> 0 us
    pallas_call x1, Pallas kernels: 246 us -> 237 us  [layer(): pl.pallas_call(functools.partial(layer_kernel, n, count, group_width), ou...]
    convert_element_type x5 -> x0, other arithmetic: 5.33 us -> none  [the longest x2 2.3 us: shards(): vg = jnp.concatenate([w_value.astype(bf), w_gate.astype(bf)], axis=1)]
where the time goes in v1:
time: 240 us
  Pallas kernels  237 us (99%)
  local copies, waits for them, and re-layouts  2.73 us (1%)
    pallas_call x1, Pallas kernels, layer(): pl.pallas_call(functools.partial(layer_kernel, n, count, group_width), ou...  237 us

profile of v1, /device:TPU:0, one launch (start us, length us, event | category | flops | bytes accessed | tf_op | source)
XLA Modules:
  0.0 240.0 jit_solution(7190087427973961928)
XLA Ops:
  0.0 237.2 %layer.1 = bf16[384,2048]{1,0:T(8,128)(2,1)} custom-call(bf16[384,2048]{1,0:T(8,128)(2,1)} %resid_hbm.1, f32[256,512]{1,0:T(8,128)} %wv_hbm.1, f32[256,512]{1,0:T(8,128)} %wg_hbm.1, f32[512,256]{1,0:T(8,128)} %wp_hbm.1, f32[256,2048]{1,0:T(8,128)} %wu_hbm.1, f32[2048,256]{1,0:T(8,128)} %wd_hbm.1, f32[1,2048]{1,0:T(1,128)} %bitcast.8, f32[1,2048]{1,0:T(1,128)} %bitcast.9, ...), custom_call_target="tpu_custom_call" | custom-call | flops 51539607552 | bytes 25165824 | tf_op jit(solution)/shard_map/layer/pallas_call | solution.py:644
  237.3 2.7 %copy.17 = bf16[384,2048]{1,0:T(8,128)(2,1)} copy(bf16[384,2048]{1,0:T(8,128)(2,1)} %layer.1) | data formatting | bytes 3145728
